TPU v7x, 32 devices: a whole 2x2x4 slice. The times are simulated.
32 devices in a mesh: ep: 4 (over y, x), tp: 8 (over z, core).
Axes of the slice: x: 2, y: 2, z: 4, core: 2. Of those that a mesh axis runs over, the one named last changes fastest.
Arguments:
- mix_tokens: bfloat16 [512, 4096], P('ep'), may hold values from -6 to 6
- mix_gain: float32 [4096], replicated, may hold values from 0.1 to 1.9
- value_weight: bfloat16 [4096, 2048], P(None, 'tp'), may hold values from -0.09375 to 0.09375
- inner_weight: bfloat16 [4096, 2048], P(None, 'tp'), may hold values from -0.09375 to 0.09375
- outer_weight: bfloat16 [4096, 2048], P(None, 'tp'), may hold values from -0.09375 to 0.09375
- conv_taps: float32 [3, 2048], P(None, 'tp'), may hold values from -3 to 3
- mix_weight: bfloat16 [2048, 4096], P('tp'), may hold values from -0.125 to 0.125
- moe_tokens: bfloat16 [512, 4096], P('ep'), may hold values from -6 to 6
- moe_gain: float32 [4096], replicated, may hold values from 0.1 to 1.9
- router_group: bfloat16 [4096, 4], replicated, may hold values from -0.09375 to 0.09375
- router_expert: bfloat16 [4096, 16], replicated, may hold values from -0.09375 to 0.09375
- expert_routes: int32 [512, 2], P('ep'), may hold values from 0 to 15, as said below
- gate_weight: bfloat16 [16, 4096, 2048], P('ep', None, 'tp'), may hold values from -0.09375 to 0.09375
- up_weight: bfloat16 [16, 4096, 2048], P('ep', None, 'tp'), may hold values from -0.09375 to 0.09375
- down_weight: bfloat16 [16, 2048, 4096], P('ep', 'tp'), may hold values from -0.5 to 0.5
Outputs:
- mixer_out: bfloat16 [512, 4096], P(('ep', 'tp'))
- expert_out: bfloat16 [512, 4096], P(('ep', 'tp'))
Inputs may be any that keep to these rules, and one draw needn't show every extreme that they name: `expert_routes`: the two experts of a row are different and lie in one group of 4 consecutive expert numbers. In each aligned block of 16 rows no expert is named more than 4 times, and in every draw some experts are named exactly 4 times in every block.
All inputs are finite; a program needn't handle non-finite values.
Results may differ from a plain program's by a relative error of at most 0.0076.
Values may be sent and summed in bfloat16 or wider, within the bound.
A program may use at most 128 MiB of HBM per device.

v0:
```python
import functools

import jax
import jax.numpy as jnp
from jax import lax
from jax.experimental import pallas as pl
from jax.experimental.pallas import tpu as pltpu
from jax.sharding import PartitionSpec as P

EPG = 4
CAP = 4
CORES = 2
CHUNKS = 8
SPLIT = (2, 2, 3, 1)
PARTS = len(SPLIT)
MESH = pl.DeviceIdType.MESH
F32, BF16 = jnp.float32, jnp.bfloat16


def iota(shape, dim):
    return lax.broadcasted_iota(jnp.int32, shape, dim)


def norm_rows(src, gain, dst):
    width = src.shape[1]

    def body(i, carry):
        rows = pl.ds(pl.multiple_of(i * 16, 16), 16)
        x = src[rows, :].astype(F32)
        inv = lax.rsqrt(jnp.sum(x * x, axis=1, keepdims=True) * (1.0 / width) + 1e-06)
        dst[rows, :] = (x * inv * gain[...]).astype(BF16)
        return carry

    lax.fori_loop(0, src.shape[0] // 16, body, 0)


def column_tiles(width, tile, body):
    def step(i, carry):
        body(pl.ds(pl.multiple_of(i * tile, tile), tile))
        return carry

    lax.fori_loop(0, width // tile, step, 0)


def kernel(
    cfg,
    mix_tokens, mix_gain, value_w, inner_w, outer_w, taps, mix_w, moe_tokens, moe_gain,
    router_group, router_expert, routes, gate_w, up_w, down_w,
    mixer_out, expert_out,
    xm, xe, rg, rx, vw, iw, ow, mw, gw, uw, dw,
    nm, ne, spread, gather, pack, got, wpack, wgot, wrow,
    gated, halo, padded, conv, ordered, pair_out, pair_in, keep, zin,
    gate_acc, up_acc, hid, both_y, y_out, y_in, y_keep, e_in, s_keep, s_out, s_in,
    load_sem, gate_sem, up_sem, down_sem,
    disp_s, disp_r, w_s, w_r, fwd_s, fwd_r, halo_s, halo_r, mp_s, mp_r, mz_s, mz_r,
    yp_s, yp_r, ye_s, ye_r, yz_s, yz_r,
):
    ep, tp, zs, half, experts_here = cfg
    e_me, t_me = lax.axis_index("ep"), lax.axis_index("tp")
    z_me, c_me = t_me // CORES, lax.rem(t_me, CORES)
    c_no = 1 - c_me
    partner = z_me * CORES + c_no
    width = xm.shape[1]
    ep_peers = [lax.rem(e_me + d, ep) for d in range(1, ep)]
    z_peers = [lax.rem(z_me + d, zs) for d in range(1, zs)]

    barrier = pltpu.get_barrier_semaphore()
    for e in ep_peers:
        pl.semaphore_signal(barrier, inc=1, device_id={"ep": e, "tp": t_me}, device_id_type=MESH)
    for z in z_peers:
        pl.semaphore_signal(
            barrier, inc=1, device_id={"ep": e_me, "tp": z * CORES + c_me}, device_id_type=MESH
        )
    pl.semaphore_signal(barrier, inc=1, device_id={"ep": e_me, "tp": partner}, device_id_type=MESH)

    def load(k, src, dst):
        return pltpu.make_async_copy(src, dst, load_sem.at[k])

    loads = [
        load(k, s, d)
        for k, (s, d) in enumerate(
            [
                (moe_tokens, xe), (router_group, rg), (router_expert, rx), (mix_tokens, xm),
                (value_w, vw), (inner_w, iw), (outer_w, ow), (mix_w, mw),
            ]
        )
    ]
    for c in loads:
        c.start()

    def remote(src, dst, s_sem, r_sem, e, t):
        return pltpu.make_async_remote_copy(
            src_ref=src, dst_ref=dst, send_sem=s_sem, recv_sem=r_sem,
            device_id={"ep": e, "tp": t}, device_id_type=MESH,
        )

    count = xe.shape[0]
    share = count // tp
    slots = half // zs
    span = ep * half
    diagonal = jnp.where(iota((count, count), 0) == iota((count, count), 1), 1.0, 0.0)
    r = lax.dot_general(
        diagonal.astype(BF16), routes[...].astype(F32).astype(BF16), (((1,), (1,)), ((), ())),
        preferred_element_type=F32,
    ).astype(jnp.int32)
    picks = [r[:, 0:1], r[:, 1:2]]
    lane = iota((count, 128), 1)
    shards = [
        sum((p >= s * experts_here).astype(jnp.int32) for s in range(1, ep)) for p in picks
    ]
    member = jnp.where((lane == shards[0]) | (lane == shards[1]), 1.0, 0.0).astype(BF16)
    ti, tj = iota((count, count), 0), iota((count, count), 1)
    earlier = jnp.where(((ti ^ tj) < share) & (tj < ti), 1.0, 0.0).astype(BF16)
    rank = jnp.dot(earlier, member, preferred_element_type=F32)
    block = lax.shift_right_logical(iota((count, 1), 0), share.bit_length() - 1)
    base = (block & 1) * span + lax.shift_right_logical(block, 1) * slots
    slot_lane = iota((count, 2 * span), 1)
    hits = []
    for s in shards:
        mine = jnp.sum(jnp.where(lane == s, rank, 0.0), axis=1, keepdims=True).astype(jnp.int32)
        hits.append(slot_lane == base + s * half + mine)
    one_hot = jnp.where(hits[0] | hits[1], 1.0, 0.0).astype(BF16)
    spread[...] = one_hot
    gather[...] = lax.dot_general(
        one_hot, diagonal.astype(BF16), (((0,), (0,)), ((), ())), preferred_element_type=F32
    ).astype(BF16)
    loads[0].wait()
    for k in range(experts_here):
        pltpu.make_async_copy(gate_w.at[k], gw.at[k], gate_sem.at[k]).start()
        pltpu.make_async_copy(up_w.at[k], uw.at[k], up_sem.at[k]).start()
    for k in range(experts_here):
        pltpu.make_async_copy(down_w.at[k], dw.at[k], down_sem.at[k]).start()
    norm_rows(xe, moe_gain, ne)
    unit = width // sum(SPLIT)

    def part_slice(q):
        return sum(SPLIT[:q]) * unit, SPLIT[q] * unit

    def pack_part(q):
        first, size = part_slice(q)
        cols = slice(first, first + size)
        pack[:, cols] = jnp.dot(
            gather[...], ne[:, cols], preferred_element_type=F32
        ).astype(BF16)

    pack_part(0)
    pl.semaphore_wait(barrier, (ep - 1) + (zs - 1) + 1)
    sends = []

    def go(copy):
        copy.start()
        sends.append(copy)

    def half_rows(c, e):
        return pl.ds(pl.multiple_of(c * span + e * half, half), half)

    def dispatch(q):
        cols = pl.ds(*part_slice(q))
        for e in ep_peers:
            go(
                remote(
                    pack.at[half_rows(c_me, e), cols], got.at[half_rows(c_me, e_me), cols],
                    disp_s.at[q, e], disp_r.at[q, e_me], e, t_me,
                )
            )

    early = PARTS // 2
    for q in range(1, PARTS):
        if q <= early:
            dispatch(q - 1)
        pack_part(q)
    loads[1].wait()
    loads[2].wait()
    lanes = (((1,), (1,)), ((), ()))
    group_exp = jnp.exp(lax.dot_general(ne[...], rg[...], lanes, preferred_element_type=F32))
    expert_logit = lax.dot_general(ne[...], rx[...], lanes, preferred_element_type=F32)
    groups, experts = group_exp.shape[1], expert_logit.shape[1]
    group = sum((picks[0] >= s * EPG).astype(jnp.int32) for s in range(1, groups))
    chosen_group = jnp.where(iota((count, groups), 1) == group, group_exp, 0.0)
    group_gate = jnp.sum(chosen_group, axis=1, keepdims=True) / jnp.sum(
        group_exp, axis=1, keepdims=True
    )
    expert_lane = iota((count, experts), 1)
    chosen = [
        jnp.exp(jnp.sum(jnp.where(expert_lane == p, expert_logit, 0.0), axis=1, keepdims=True))
        for p in picks
    ]
    scale = chosen[0] + chosen[1]
    weights = sum(
        jnp.where(lane == p, group_gate * c / scale, 0.0) for p, c in zip(picks, chosen)
    )
    parts, rest = [], weights
    for _ in range(3):
        parts.append(rest.astype(BF16))
        rest = rest - parts[-1].astype(F32)
    packed_w = sum(jnp.dot(gather[...], p, preferred_element_type=F32) for p in parts)
    for e in range(ep):
        for c in range(CORES):
            wpack[e, c * half : (c + 1) * half, :] = packed_w[
                c * span + e * half : c * span + (e + 1) * half, :
            ]
    wgot[e_me] = wpack[e_me]
    for c in range(CORES):
        got[half_rows(c, e_me), :] = pack[half_rows(c, e_me), :]

    loads[3].wait()
    norm_rows(xm, mix_gain, nm)
    loads[4].wait()
    loads[5].wait()
    rows = xm.shape[0]
    value_proj = jnp.dot(nm[...], vw[...], preferred_element_type=F32)
    inner_proj = jnp.dot(nm[...], iw[...], preferred_element_type=F32)
    gated[...] = (inner_proj * value_proj).astype(BF16)
    halo_copy = remote(
        gated.at[pl.ds(rows - 16, 16), :], halo, halo_s.at[0], halo_r.at[0],
        lax.rem(e_me + 1, ep), t_me,
    )
    halo_copy.start()
    for q in range(early, PARTS):
        dispatch(q)
        if q == early:
            for e in ep_peers:
                go(remote(wpack.at[e], wgot.at[e_me], w_s.at[e], w_r.at[e_me], e, t_me))
    padded[8:, :] = gated[...].astype(F32)
    loads[6].wait()
    outer_proj = jnp.dot(nm[...], ow[...], preferred_element_type=F32)
    mix_share = rows // tp
    mix_rows = zs * mix_share
    everything = slice(None)
    pair_copy = remote(pair_out, pair_in, mp_s.at[0], mp_r.at[0], e_me, partner)

    def parity_rows(ref, c, step, cols):
        return jnp.concatenate(
            [
                ref[pl.ds(pl.multiple_of((z * CORES + c) * step, step), step), cols]
                for z in range(zs)
            ],
            axis=0,
        )

    def z_rows(z, step):
        return pl.ds(pl.multiple_of(z * step, step), step)

    def mixer_pair():
        halo_copy.wait()
        before = halo[...].astype(F32)[8:16, :]
        padded[0:8, :] = jnp.where(e_me > 0, before, jnp.zeros_like(before))
        n_taps = taps.shape[0]
        mixed = taps[0:1, :] * padded[pl.ds(9 - n_taps, rows), :]
        for j in range(1, n_taps):
            mixed = mixed + taps[j : j + 1, :] * padded[pl.ds(9 - n_taps + j, rows), :]
        conv[...] = (outer_proj * mixed).astype(BF16)

        loads[7].wait()

        ordered[0:mix_rows, :] = parity_rows(conv, c_no, mix_share, everything)
        ordered[mix_rows:, :] = parity_rows(conv, c_me, mix_share, everything)

        def mix_tile(cols):
            both = jnp.dot(ordered[...], mw[:, cols], preferred_element_type=F32)
            pair_out[:, cols] = both[0:mix_rows].astype(BF16)
            keep[:, cols] = both[mix_rows:]

        column_tiles(width, 512, mix_tile)
        go(pair_copy)

    def mixer_sums():
        pair_copy.wait_recv()

        def sum_tile(cols):
            total = keep[:, cols] + pair_in[:, cols].astype(F32)
            keep[:, cols] = total
            pair_in[:, cols] = total.astype(BF16)

        column_tiles(width, 512, sum_tile)

        for z in z_peers:
            go(
                remote(
                    pair_in.at[z_rows(z, mix_share), :], zin.at[z_me], mz_s.at[z], mz_r.at[z_me],
                    e_me, z * CORES + c_me,
                )
            )

    def forward(q):
        cols = pl.ds(*part_slice(q))
        for e in ep_peers:
            here = got.at[half_rows(c_me, e), cols]
            remote(here, here, disp_s.at[q, e], disp_r.at[q, e], e, t_me).wait_recv()
            go(remote(here, here, fwd_s.at[q, e], fwd_r.at[q, e], e_me, partner))

    def forwarded(q):
        cols = pl.ds(*part_slice(q))
        for e in ep_peers:
            there = got.at[half_rows(c_no, e), cols]
            remote(there, there, fwd_s.at[q, e], fwd_r.at[q, e], e_me, partner).wait_recv()

    arrived_lane = iota((2 * span, 128), 1)

    def project(q):
        first, size = part_slice(q)
        cols = slice(first, first + size)

        def expert(k, carry):
            gate = jnp.dot(got[:, cols], gw[k, cols, :], preferred_element_type=F32)
            up = jnp.dot(got[:, cols], uw[k, cols, :], preferred_element_type=F32)
            if q:
                gate = gate + gate_acc[k]
                up = up + up_acc[k]
            if q < PARTS - 1:
                gate_acc[k] = gate
                up_acc[k] = up
                return carry
            weight = jnp.sum(
                jnp.where(arrived_lane == e_me * experts_here + k, wrow[...], 0.0),
                axis=1, keepdims=True,
            )
            hid[k] = (gate / (1.0 + jnp.exp(-gate)) * up * weight).astype(BF16)
            return carry

        lax.fori_loop(0, experts_here, expert, 0)

    forward(0)
    for k in range(experts_here):
        pltpu.make_async_copy(gate_w.at[k], gw.at[k], gate_sem.at[k]).wait()
        pltpu.make_async_copy(up_w.at[k], uw.at[k], up_sem.at[k]).wait()
    for q in range(PARTS):
        if q + 1 < PARTS:
            forward(q + 1)
            if q == 1:
                mixer_sums()
        else:
            for e in ep_peers:
                remote(wgot.at[e], wgot.at[e], w_s.at[e], w_r.at[e], e, t_me).wait_recv()
            for c in range(CORES):
                for e in range(ep):
                    wrow[c * span + e * half : c * span + (e + 1) * half, :] = wgot[
                        e, c * half : (c + 1) * half, :
                    ]
        forwarded(q)
        project(q)
        if q == 0:
            mixer_pair()
    for k in range(experts_here):
        pltpu.make_async_copy(down_w.at[k], dw.at[k], down_sem.at[k]).wait()

    chunk = width // CHUNKS
    tile = min(512, chunk)

    def core_rows(c):
        return pl.ds(pl.multiple_of(c * span, span), span)

    y_copies = {}

    def stage_a(j):
        for i in range(chunk // tile):
            at = slice(i * tile, (i + 1) * tile)
            cols = slice(j * chunk + i * tile, j * chunk + (i + 1) * tile)
            both = jnp.dot(hid[0], dw[0, :, cols], preferred_element_type=F32)
            for k in range(1, experts_here):
                both = both + jnp.dot(hid[k], dw[k, :, cols], preferred_element_type=F32)
            both_y[...] = both
            y_out[j, :, at] = both_y[core_rows(c_no), :].astype(BF16)
            y_keep[j % 3, :, at] = both_y[core_rows(c_me), :]
        y_copies[j] = remote(y_out.at[j], y_in.at[j], yp_s.at[j], yp_r.at[j], e_me, partner)
        go(y_copies[j])

    def e_rows(e):
        return pl.ds(pl.multiple_of(e * half, half), half)

    def stage_b(j):
        y_copies[j].wait_recv()
        y_in[j] = (y_keep[j % 3] + y_in[j].astype(F32)).astype(BF16)
        for e in ep_peers:
            go(
                remote(
                    y_in.at[j, e_rows(e), :], e_in.at[j, e_rows(e_me), :],
                    ye_s.at[j, e], ye_r.at[j, e_me], e, t_me,
                )
            )
        e_in[j, e_rows(e_me), :] = y_in[j, e_rows(e_me), :]

    def stage_c(j):
        for e in ep_peers:
            here = e_in.at[j, e_rows(e), :]
            remote(here, here, ye_s.at[j, e], ye_r.at[j, e], e, t_me).wait_recv()
        own = parity_rows(spread, c_me, share, core_rows(c_me))
        total = jnp.dot(own, e_in[j], preferred_element_type=F32)
        s_out[j] = total.astype(BF16)
        for z in z_peers:
            go(
                remote(
                    s_out.at[j, z_rows(z, share), :], s_in.at[j, z_me],
                    yz_s.at[j, z], yz_r.at[j, z_me], e_me, z * CORES + c_me,
                )
            )
        s_keep[j % 4] = total

    def stage_d(j):
        total = s_keep[j % 4, z_rows(z_me, share), :]
        for z in z_peers:
            here = s_in.at[j, z]
            remote(here, here, yz_s.at[j, z], yz_r.at[j, z], e_me, z * CORES + c_me).wait_recv()
            total = total + s_in[j, z].astype(F32)
        expert_out[:, j * chunk : (j + 1) * chunk] = total.astype(BF16)

    def mixer_final():
        total = keep[z_rows(z_me, mix_share), :]
        for z in z_peers:
            here = zin.at[z]
            remote(here, here, mz_s.at[z], mz_r.at[z], e_me, z * CORES + c_me).wait_recv()
            total = total + zin[z].astype(F32)
        mixer_out[...] = total.astype(BF16)

    lag_b, lag_c, lag_d = 2, 7, 10
    for step in range(CHUNKS + lag_d):
        for stage, lag in ((stage_a, 0), (stage_b, lag_b), (stage_c, lag_c), (stage_d, lag_d)):
            if 0 <= step - lag < CHUNKS:
                stage(step - lag)
        if step == CHUNKS:
            mixer_final()

    for copy in sends:
        copy.wait_send()


def store(a, b, a_out, b_out, held, sem):
    refs = ((a, a_out), (b, b_out))
    into = [pltpu.make_async_copy(s, held.at[i], sem.at[0, i]) for i, (s, _) in enumerate(refs)]
    outof = [pltpu.make_async_copy(held.at[i], d, sem.at[1, i]) for i, (_, d) in enumerate(refs)]
    for c in into:
        c.start()
    for c, d in zip(into, outof):
        c.wait()
        d.start()
    for d in outof:
        d.wait()


def local(ep, tp, *args):
    (mix_tokens, mix_gain, value_w, inner_w, outer_w, taps, mix_w, moe_tokens, moe_gain,
     router_group, router_expert, routes, gate_w, up_w, down_w) = args
    rows, width = mix_tokens.shape
    count = moe_tokens.shape[0]
    channels, hidden = value_w.shape[1], gate_w.shape[2]
    experts_here = gate_w.shape[0]
    zs = tp // CORES
    share, mix_share = count // tp, rows // tp
    topk = routes.shape[1]
    slots = experts_here * CAP
    if experts_here % EPG == 0:
        slots = slots // topk
    slots = min(slots, share)
    half = zs * slots
    span = ep * half
    chunk = width // CHUNKS
    any_ref = pl.BlockSpec(memory_space=pl.ANY)
    vmem = pl.BlockSpec(memory_space=pltpu.VMEM)
    V, D = pltpu.VMEM, lambda *s: pltpu.SemaphoreType.DMA(s)
    scratch = [
        V((rows, width), BF16), V((count, width), BF16),
        V(router_group.T.shape, BF16), V(router_expert.T.shape, BF16),
        V(value_w.shape, BF16), V(inner_w.shape, BF16), V(outer_w.shape, BF16),
        V(mix_w.shape, BF16),
        V(gate_w.shape, BF16), V(up_w.shape, BF16), V(down_w.shape, BF16),
        V((rows, width), BF16), V((count, width), BF16), V((count, 2 * span), BF16), V((2 * span, count), BF16),
        V((2 * span, width), BF16), V((2 * span, width), BF16),
        V((ep, 2 * half, 128), F32), V((ep, 2 * half, 128), F32), V((2 * span, 128), F32),
        V((rows, channels), BF16), V((16, channels), BF16), V((rows + 8, channels), F32),
        V((rows, channels), BF16), V((rows, channels), BF16),
        V((zs * mix_share, width), BF16), V((zs * mix_share, width), BF16),
        V((zs * mix_share, width), F32),
        V((zs, mix_share, width), BF16),
        V((experts_here, 2 * span, hidden), F32), V((experts_here, 2 * span, hidden), F32),
        V((experts_here, 2 * span, hidden), BF16), V((2 * span, min(512, chunk)), F32),
        V((CHUNKS, span, chunk), BF16), V((CHUNKS, span, chunk), BF16),
        V((3, span, chunk), F32),
        V((CHUNKS, span, chunk), BF16),
        V((4, zs * share, chunk), F32), V((CHUNKS, zs * share, chunk), BF16),
        V((CHUNKS, zs, share, chunk), BF16),
        D(8), D(experts_here), D(experts_here), D(experts_here),
        D(PARTS, ep), D(PARTS, ep), D(ep), D(ep), D(PARTS, ep), D(PARTS, ep), D(1), D(1), D(1), D(1), D(zs), D(zs),
        D(CHUNKS), D(CHUNKS), D(CHUNKS, ep), D(CHUNKS, ep), D(CHUNKS, zs), D(CHUNKS, zs),
    ]
    out = [
        jax.ShapeDtypeStruct((mix_share, width), BF16),
        jax.ShapeDtypeStruct((share, width), BF16),
    ]
    in_specs = [
        any_ref, vmem, any_ref, any_ref, any_ref, vmem, any_ref, any_ref, vmem,
        any_ref, any_ref, vmem, any_ref, any_ref, any_ref,
    ]
    results = pl.pallas_call(
        functools.partial(kernel, (ep, tp, zs, half, experts_here)),
        out_shape=out,
        in_specs=in_specs,
        out_specs=[vmem, vmem],
        scratch_shapes=scratch,
        compiler_params=pltpu.CompilerParams(
            collective_id=0, has_side_effects=True, vmem_limit_bytes=67043328
        ),
        name="mixer_and_experts",
    )(
        mix_tokens, mix_gain.reshape(1, width), value_w, inner_w, outer_w, taps, mix_w,
        moe_tokens, moe_gain.reshape(1, width), router_group.T, router_expert.T, routes.T,
        gate_w, up_w, down_w,
    )
    return pl.pallas_call(
        store,
        out_shape=out,
        in_specs=[any_ref, any_ref],
        out_specs=[any_ref, any_ref],
        scratch_shapes=[V((2, share, width), BF16), D(2, 2)],
        name="store",
    )(*results)


def solution(mesh):
    return jax.shard_map(
        lambda *args: tuple(local(mesh.shape["ep"], mesh.shape["tp"], *args)),
        mesh=mesh,
        in_specs=(
            P("ep", None), P(), P(None, "tp"), P(None, "tp"), P(None, "tp"), P(None, "tp"),
            P("tp", None), P("ep", None), P(), P(), P(), P("ep", None),
            P("ep", None, "tp"), P("ep", None, "tp"), P("ep", "tp", None),
        ),
        out_specs=(P(("ep", "tp"), None), P(("ep", "tp"), None)),
        check_vma=False,
    )
```

profile of v0, /device:TPU:0, one launch (start us, length us, event | category | flops | bytes accessed | tf_op | source)
XLA Modules:
  0.0 50.6 jit_solution(14560396808444789388)
XLA Ops:
  0.6 48.3 %mixer_and_experts.1 = (bf16[16,4096]{1,0:T(8,128)(2,1)}, bf16[16,4096]{1,0:T(8,128)(2,1)}) custom-call(bf16[128,4096]{1,0:T(8,128)(2,1)} %mix_tokens.1, f32[1,4096]{1,0:T(1,128)} %bitcast.7, bf16[4096,256]{1,0:T(8,128)(2,1)} %value_w.1, bf16[4096,256]{1,0:T(8,128)(2,1)} %inner_w.1, bf16[4096,256]{1,0:T(8,128)(2,1)} %outer_w.1, f32[3,256]{1,0:T(4,128)} %taps.1, ...), custom_call_target="tpu_custom_call" | custom-call | tf_op jit(solution)/shard_map/mixer_and_experts/pallas_call | solution.py:493
  49.0 1.7 %store.1 = (bf16[16,4096]{1,0:T(8,128)(2,1)}, bf16[16,4096]{1,0:T(8,128)(2,1)}) custom-call(bf16[16,4096]{1,0:T(8,128)(2,1)} %get-tuple-element.4.a, bf16[16,4096]{1,0:T(8,128)(2,1)} %get-tuple-element.5.b), custom_call_target="tpu_custom_call" | custom-call | tf_op jit(solution)/shard_map/store/pallas_call | solution.py:508
where the time goes:
time: 50.8 us; the launch traced here: 50.6 us
  Pallas kernels  50 us (98%)
  between operations  0.64 us (1%)
    pallas_call x1, Pallas kernels, local(): pl.pallas_call(functools.partial(kernel, (ep, tp, zs, half, experts_here)...  48.3 us
    pallas_call x1, Pallas kernels, local(): pl.pallas_call(store, out_shape=out, in_specs=[any_ref, any_ref], out_spe...  1.66 us

commit v1 on v0

v1 whole, which is shorter than its diff:
```python
import functools

import jax
import jax.numpy as jnp
from jax import lax
from jax.experimental import pallas as pl
from jax.experimental.pallas import tpu as pltpu
from jax.sharding import PartitionSpec as P

EPG = 4
CAP = 4
CORES = 2
CHUNKS = (1, 2, 2, 2, 2, 2, 2, 2, 1)
LAGS = (2, 8, 2, 3)
DIRECT = 2
SPLIT = (2, 2, 3, 1)
PARTS = len(SPLIT)
MESH = pl.DeviceIdType.MESH
F32, BF16 = jnp.float32, jnp.bfloat16


def iota(shape, dim):
    return lax.broadcasted_iota(jnp.int32, shape, dim)


def norm_rows(src, gain, dst):
    width = src.shape[1]

    def body(i, carry):
        rows = pl.ds(pl.multiple_of(i * 16, 16), 16)
        x = src[rows, :].astype(F32)
        inv = lax.rsqrt(jnp.sum(x * x, axis=1, keepdims=True) * (1.0 / width) + 1e-06)
        dst[rows, :] = (x * inv * gain[...]).astype(BF16)
        return carry

    lax.fori_loop(0, src.shape[0] // 16, body, 0, unroll=4)


def row_scales(src):
    width = src.shape[1]
    total = None
    for first in range(0, width, 512):
        x = src[:, first : first + 512].astype(F32)
        square = x * x
        total = square if total is None else total + square
    return lax.rsqrt(jnp.sum(total, axis=1, keepdims=True) * (1.0 / width) + 1e-06)


def column_tiles(width, tile, body):
    def step(i, carry):
        body(pl.ds(pl.multiple_of(i * tile, tile), tile))
        return carry

    lax.fori_loop(0, width // tile, step, 0)


def kernel(
    cfg,
    mix_tokens, mix_gain_in, value_w, inner_w, outer_w, taps_in, mix_w, moe_tokens, moe_gain_in,
    router_group, router_expert, routes_in, gate_w, up_w, down_w,
    mixer_out, expert_out,
    mix_gain, taps, moe_gain, routes, xm, xe, rg, rx, vw, iw, ow, mw, gw, uw, dw,
    nm, ne, spread, gather, pack, got, wpack, wgot, wrow,
    gated, halo, padded, conv, ordered, pair_out, pair_in, keep, zin,
    gate_acc, up_acc, hid, both_y, y_out, y_in, y_keep, e_in, s_keep, s_out, s_in,
    load_sem, expert_sem, down_sem,
    near_s, near_r, far_s, far_r, rel_s, rel_r, w_s, w_r, fwd_s, fwd_r, halo_s, halo_r,
    mp_s, mp_r, mz_s, mz_r, yp_s, yp_r, ye_s, ye_r, yz_s, yz_r,
):
    ep, side, tp, zs, half, experts_here, w_rows = cfg
    e_me, t_me = lax.axis_index("ep"), lax.axis_index("tp")
    z_me, c_me = t_me // CORES, lax.rem(t_me, CORES)
    c_no = 1 - c_me
    partner = z_me * CORES + c_no
    width = xm.shape[1]
    tall = ep // side
    e_row, e_col = e_me // side, lax.rem(e_me, side)

    def placed(down, across):
        return lax.rem(e_row + down, tall) * side + lax.rem(e_col + across, side)

    near = [placed(d, 0) for d in range(1, tall)] + [placed(0, a) for a in range(1, side)]
    far = [placed(d, a) for d in range(1, tall) for a in range(1, side)]
    ep_peers = near + far
    z_odd = lax.rem(z_me, 2)
    z_pair = z_me + 1 - 2 * z_odd
    z_peers = [lax.rem(z_me + d, zs) for d in range(1, zs)]

    def start(copy):
        copy.start()

    barrier = pltpu.get_barrier_semaphore()
    for e in ep_peers:
        pl.semaphore_signal(barrier, inc=1, device_id={"ep": e, "tp": t_me}, device_id_type=MESH)
    for z in z_peers:
        pl.semaphore_signal(
            barrier, inc=1, device_id={"ep": e_me, "tp": z * CORES + c_me}, device_id_type=MESH
        )
    pl.semaphore_signal(barrier, inc=1, device_id={"ep": e_me, "tp": partner}, device_id_type=MESH)

    def load(k, src, dst):
        return pltpu.make_async_copy(src, dst, load_sem.at[k])

    loads = [
        load(k, s, d)
        for k, (s, d) in enumerate(
            [
                (moe_tokens, xe), (router_group, rg), (router_expert, rx), (mix_tokens, xm),
                (value_w, vw), (inner_w, iw), (outer_w, ow), (mix_w, mw),
                (routes_in, routes), (moe_gain_in, moe_gain), (mix_gain_in, mix_gain), (taps_in, taps),
            ]
        )
    ]
    unit = width // sum(SPLIT)

    def part_slice(q):
        return sum(SPLIT[:q]) * unit, SPLIT[q] * unit

    def expert_loads(q):
        rows = pl.ds(*part_slice(q))
        return [
            pltpu.make_async_copy(gate_w.at[:, rows, :], gw.at[:, rows, :], expert_sem.at[q]),
            pltpu.make_async_copy(up_w.at[:, rows, :], uw.at[:, rows, :], expert_sem.at[q]),
        ]

    hidden = down_w.shape[1]
    down_loads = [
        pltpu.make_async_copy(
            down_w.at[k], dw.at[k * hidden : (k + 1) * hidden, :], down_sem
        )
        for k in range(experts_here)
    ]
    for k in (8, 0, 9, 3, 10, 4, 5):
        loads[k].start()

    def remote(src, dst, s_sem, r_sem, e, t):
        return pltpu.make_async_remote_copy(
            src_ref=src, dst_ref=dst, send_sem=s_sem, recv_sem=r_sem,
            device_id={"ep": e, "tp": t}, device_id_type=MESH,
        )

    count = xe.shape[0]
    share = count // tp
    slots = half // zs
    span = ep * half
    loads[8].wait()
    diagonal = jnp.where(iota((count, count), 0) == iota((count, count), 1), 1.0, 0.0)
    r = lax.dot_general(
        diagonal.astype(BF16), routes[...].astype(F32).astype(BF16), (((1,), (1,)), ((), ())),
        preferred_element_type=F32,
    ).astype(jnp.int32)
    picks = [r[:, 0:1], r[:, 1:2]]
    lane = iota((count, -(-ep * w_rows // 128) * 128), 1)
    shards = [
        sum((p >= s * experts_here).astype(jnp.int32) for s in range(1, ep)) for p in picks
    ]
    member = jnp.where((lane == shards[0]) | (lane == shards[1]), 1.0, 0.0).astype(BF16)
    ti, tj = iota((count, count), 0), iota((count, count), 1)
    earlier = jnp.where(((ti ^ tj) < share) & (tj < ti), 1.0, 0.0).astype(BF16)
    rank = jnp.dot(earlier, member, preferred_element_type=F32)
    block = lax.shift_right_logical(iota((count, 1), 0), share.bit_length() - 1)
    base = (block & 1) * span + lax.shift_right_logical(block, 1) * slots
    slot_lane = iota((count, 2 * span), 1)
    hits = []
    for s in shards:
        mine = jnp.sum(jnp.where(lane == s, rank, 0.0), axis=1, keepdims=True).astype(jnp.int32)
        hits.append(slot_lane == base + s * half + mine)
    one_hot = jnp.where(hits[0] | hits[1], 1.0, 0.0).astype(BF16)
    spread[...] = one_hot
    gather[...] = lax.dot_general(
        one_hot, diagonal.astype(BF16), (((0,), (0,)), ((), ())), preferred_element_type=F32
    ).astype(BF16)
    loads[0].wait()
    loads[9].wait()

    def pack_part(q):
        first, size = part_slice(q)
        cols = slice(first, first + size)
        ne[:, cols] = (xe[:, cols].astype(F32) * moe_gain[:, cols]).astype(BF16)
        pack[:, cols] = jnp.dot(
            gather[...], ne[:, cols], preferred_element_type=F32
        ).astype(BF16)

    pack_part(0)
    pack_part(1)
    for k in (1, 2, 6, 11, 7):
        loads[k].start()
    for c in expert_loads(0):
        c.start()
    pl.semaphore_wait(barrier, (ep - 1) + (zs - 1) + 1)
    def half_rows(c, e):
        return pl.ds(pl.multiple_of(c * span + e * half, half), half)

    def half_cols(q, odd):
        first, size = part_slice(q)
        return pl.ds(pl.multiple_of(first + odd * (size // 2), 128), size // 2)

    def dispatch(q, peers, cols, s_sem, r_sem):
        for e in peers:
            start(
                remote(
                    pack.at[half_rows(c_me, e), cols], got.at[half_rows(c_me, e_me), cols],
                    s_sem, r_sem.at[q], e, t_me,
                )
            )

    def dispatch_far(q):
        dispatch(q, far, half_cols(q, z_odd), far_s, far_r)

    def dispatch_near(q):
        dispatch(q, near, pl.ds(*part_slice(q)), near_s, near_r)

    def landed(count, size, sem):
        here = got.at[pl.ds(0, count * half), pl.ds(0, size)]
        remote(here, here, sem, sem, e_me, partner).wait_recv()

    def forward(q, e, cols):
        here = got.at[half_rows(c_me, e), cols]
        start(remote(here, here, fwd_s, fwd_r.at[q], e_me, partner))

    def relay(q):
        cols = half_cols(q, z_odd)
        landed(len(far), part_slice(q)[1] // 2, far_r.at[q])
        for e in far:
            here = got.at[half_rows(c_me, e), cols]
            start(remote(here, here, rel_s, rel_r.at[q], e_me, z_pair * CORES + c_me))
            forward(q, e, cols)

    def forward_near(q):
        landed(len(near), part_slice(q)[1], near_r.at[q])
        for e in near:
            forward(q, e, pl.ds(*part_slice(q)))

    def forward_far(q):
        landed(len(far), part_slice(q)[1] // 2, rel_r.at[q])
        for e in far:
            forward(q, e, half_cols(q, 1 - z_odd))

    def forwarded(q):
        landed(ep - 1, part_slice(q)[1], fwd_r.at[q])

    dispatch_far(0)
    dispatch_near(0)
    loads[3].wait()
    loads[10].wait()
    norm_rows(xm, mix_gain, nm)
    loads[4].wait()
    loads[5].wait()
    rows = xm.shape[0]
    value_proj = jnp.dot(nm[...], vw[...], preferred_element_type=F32)
    inner_proj = jnp.dot(nm[...], iw[...], preferred_element_type=F32)
    gated[...] = (inner_proj * value_proj).astype(BF16)
    halo_copy = remote(
        gated.at[pl.ds(rows - 16, 16), :], halo, halo_s, halo_r,
        lax.rem(e_me + 1, ep), t_me,
    )
    halo_copy.start()
    dispatch_far(1)
    for q in range(1, PARTS):
        for c in expert_loads(q):
            c.start()
    for q in range(2, PARTS):
        pack_part(q)
        dispatch_far(q)
        dispatch_near(q - 1)
    loads[1].wait()
    loads[2].wait()
    lanes = (((1,), (1,)), ((), ()))
    row_scale = row_scales(xe)
    group_exp = jnp.exp(
        row_scale * lax.dot_general(ne[...], rg[...], lanes, preferred_element_type=F32)
    )
    expert_logit = row_scale * lax.dot_general(
        ne[...], rx[...], lanes, preferred_element_type=F32
    )
    groups, experts = group_exp.shape[1], expert_logit.shape[1]
    group = sum((picks[0] >= s * EPG).astype(jnp.int32) for s in range(1, groups))
    chosen_group = jnp.where(iota((count, groups), 1) == group, group_exp, 0.0)
    group_gate = jnp.sum(chosen_group, axis=1, keepdims=True) / jnp.sum(
        group_exp, axis=1, keepdims=True
    )
    expert_lane = iota((count, experts), 1)
    chosen = [
        jnp.exp(jnp.sum(jnp.where(expert_lane == p, expert_logit, 0.0), axis=1, keepdims=True))
        for p in picks
    ]
    scale = chosen[0] + chosen[1]
    w_lanes = [s * w_rows + (p - s * experts_here) for s, p in zip(shards, picks)]
    weights = sum(
        jnp.where(lane == at, group_gate * c / scale, 0.0) for at, c in zip(w_lanes, chosen)
    )
    scale_lanes = [s * w_rows + experts_here for s in shards]
    weights = weights + jnp.where(
        (lane == scale_lanes[0]) | (lane == scale_lanes[1]), row_scale, 0.0
    )

    def three_parts(value):
        parts = []
        for _ in range(3):
            parts.append(value.astype(BF16))
            value = value - parts[-1].astype(F32)
        return parts

    packed_w = sum(
        lax.dot_general(p, spread[...], (((0,), (0,)), ((), ())), preferred_element_type=F32)
        for p in three_parts(weights)
    )
    for e in range(ep):
        for c in range(CORES):
            wpack[e, :, c * half : (c + 1) * half] = packed_w[
                e * w_rows : (e + 1) * w_rows, c * span + e * half : c * span + (e + 1) * half
            ]
    wgot[e_me] = wpack[e_me]
    for c in range(CORES):
        got[half_rows(c, e_me), :] = pack[half_rows(c, e_me), :]

    for e in ep_peers:
        start(remote(wpack.at[e], wgot.at[e_me], w_s, w_r, e, t_me))
    dispatch_near(PARTS - 1)
    padded[8:, :] = gated[...].astype(F32)
    loads[6].wait()
    outer_proj = jnp.dot(nm[...], ow[...], preferred_element_type=F32)
    mix_share = rows // tp
    mix_rows = zs * mix_share
    everything = slice(None)
    pair_copy = remote(pair_out, pair_in, mp_s, mp_r, e_me, partner)

    def parity_rows(ref, c, step, cols):
        return jnp.concatenate(
            [
                ref[pl.ds(pl.multiple_of((z * CORES + c) * step, step), step), cols]
                for z in range(zs)
            ],
            axis=0,
        )

    def z_rows(z, step):
        return pl.ds(pl.multiple_of(z * step, step), step)

    steps = zs.bit_length() - 1

    def z_partner(s):
        return z_me + (1 - 2 * lax.rem(z_me // 2**s, 2)) * 2**s

    def z_owners(z, s):
        low = lax.rem(z, 2 ** (s + 1))
        return [low + m * 2 ** (s + 1) for m in range(zs >> (s + 1))]

    def z_slot(s):
        return sum(zs >> (t + 1) for t in range(s))

    def z_send(s, src, dst, step, cols, s_sem, r_sem):
        to = z_partner(s)
        for m, owner in enumerate(z_owners(to, s)):
            start(
                remote(
                    src.at[z_rows(owner, step), cols], dst.at[z_slot(s) + m, :, cols],
                    s_sem, r_sem, e_me, to * CORES + c_me,
                )
            )

    def z_landed(blocks, ref, size, sem):
        here = ref.at[pl.ds(0, blocks), :, pl.ds(0, size)]
        remote(here, here, sem, sem, e_me, partner).wait_recv()

    def mixer_pair():
        halo_copy.wait()
        before = halo[...].astype(F32)[8:16, :]
        padded[0:8, :] = jnp.where(e_me > 0, before, jnp.zeros_like(before))
        loads[11].wait()
        n_taps = taps.shape[0]
        mixed = taps[0:1, :] * padded[pl.ds(9 - n_taps, rows), :]
        for j in range(1, n_taps):
            mixed = mixed + taps[j : j + 1, :] * padded[pl.ds(9 - n_taps + j, rows), :]
        conv[...] = (outer_proj * mixed).astype(BF16)

        loads[7].wait()

        ordered[0:mix_rows, :] = parity_rows(conv, c_no, mix_share, everything)
        ordered[mix_rows:, :] = parity_rows(conv, c_me, mix_share, everything)

        def mix_tile(cols):
            both = jnp.dot(ordered[...], mw[:, cols], preferred_element_type=F32)
            pair_out[:, cols] = both[0:mix_rows].astype(BF16)
            keep[:, cols] = both[mix_rows:]

        column_tiles(width, 512, mix_tile)
        pair_copy.start()

    def mixer_sums():
        pair_copy.wait_recv()

        def sum_tile(cols):
            total = keep[:, cols] + pair_in[:, cols].astype(F32)
            keep[:, cols] = total
            pair_in[:, cols] = total.astype(BF16)

        column_tiles(width, 512, sum_tile)

        z_send(0, pair_in, zin, mix_share, pl.ds(0, width), mz_s, mz_r.at[0])

    def mixer_step(s):
        z_landed(zs >> s, zin, width, mz_r.at[s - 1])
        for m, owner in enumerate(z_owners(z_me, s - 1)):
            rows = z_rows(owner, mix_share)
            total = keep[rows, :] + zin[z_slot(s - 1) + m].astype(F32)
            keep[rows, :] = total
            pair_in[rows, :] = total.astype(BF16)
        z_send(s, pair_in, zin, mix_share, pl.ds(0, width), mz_s, mz_r.at[s])

    def project(q):
        first, size = part_slice(q)
        cols = slice(first, first + size)

        for k in range(experts_here):
            gate = jnp.dot(got[:, cols], gw[k, cols, :], preferred_element_type=F32)
            up = jnp.dot(got[:, cols], uw[k, cols, :], preferred_element_type=F32)
            if q:
                gate = gate + gate_acc[k]
                up = up + up_acc[k]
            if q < PARTS - 1:
                gate_acc[k] = gate
                up_acc[k] = up
                continue
            row = wrow[:, experts_here : experts_here + 1]
            gate = gate * row
            hid[:, k * hidden : (k + 1) * hidden] = (gate / (1.0 + jnp.exp(-gate)) * up * (row * wrow[:, k : k + 1])).astype(BF16)

    def arrived_weights():
        arrived = wgot.at[pl.ds(0, ep - 1)]
        remote(arrived, arrived, w_s, w_r, e_me, partner).wait_recv()
        across = jnp.concatenate(
            [wgot[e, :, c * half : (c + 1) * half] for c in range(CORES) for e in range(ep)], axis=1
        )
        square = (2 * span, 2 * span)
        same = jnp.where(iota(square, 0) == iota(square, 1), 1.0, 0.0).astype(BF16)
        wrow[...] = sum(
            lax.dot_general(same, p, lanes, preferred_element_type=F32)
            for p in three_parts(across)
        )

    for c in down_loads:
        c.start()
    relay(0)
    forward_near(0)
    relay(1)
    mixer_pair()
    forward_far(0)
    for q in range(PARTS):
        if q == 1:
            for later in range(2, PARTS):
                relay(later)
            mixer_sums()
        if q == 2:
            arrived_weights()
        if q == 3:
            mixer_step(1)
        if 0 < q and q + 1 < PARTS:
            forward_near(q + 1)
            forward_far(q + 1)
        both_parts = gw.at[:, pl.ds(0, 2 * part_slice(q)[1]), :]
        pltpu.make_async_copy(both_parts, both_parts, expert_sem.at[q]).wait()
        forwarded(q)
        project(q)
        if q == 0:
            forward_near(1)
            forward_far(1)
    pltpu.make_async_copy(dw, dw, down_sem).wait()

    chunk_unit = width // sum(CHUNKS)

    def chunk_cols(j):
        return slice(sum(CHUNKS[:j]) * chunk_unit, sum(CHUNKS[: j + 1]) * chunk_unit)

    def core_rows(c):
        return pl.ds(pl.multiple_of(c * span, span), span)

    y_copies = {}

    def stage_a(j):
        cols = chunk_cols(j)
        size = cols.stop - cols.start
        both_y[:, 0:size] = jnp.dot(hid[...], dw[:, cols], preferred_element_type=F32)
        y_out[:, cols] = both_y[core_rows(c_no), 0:size].astype(BF16)
        y_keep[:, cols] = both_y[core_rows(c_me), 0:size]
        y_copies[j] = remote(
            y_out.at[:, cols], y_in.at[:, cols], yp_s, yp_r.at[j], e_me, partner
        )
        y_copies[j].start()

    def e_rows(e):
        return pl.ds(pl.multiple_of(e * half, half), half)

    def stage_b(j):
        cols = chunk_cols(j)
        y_copies[j].wait_recv()
        y_in[:, cols] = (y_keep[:, cols] + y_in[:, cols].astype(F32)).astype(BF16)
        for e in ep_peers:
            start(
                remote(
                    y_in.at[e_rows(e), cols], e_in.at[e_rows(e_me), cols],
                    ye_s, ye_r.at[j], e, t_me,
                )
            )
        e_in[e_rows(e_me), cols] = y_in[e_rows(e_me), cols]

    def direct(j):
        return j >= len(CHUNKS) - DIRECT

    def stage_c(j):
        cols = chunk_cols(j)
        size = cols.stop - cols.start
        here = e_in.at[pl.ds(0, (ep - 1) * half), pl.ds(0, size)]
        remote(here, here, ye_s, ye_r.at[j], e_me, partner).wait_recv()
        own = parity_rows(spread, c_me, share, core_rows(c_me))
        total = jnp.dot(own, e_in[:, cols], preferred_element_type=F32)
        s_out[:, cols] = total.astype(BF16)
        if direct(j):
            for z in z_peers:
                start(
                    remote(
                        s_out.at[z_rows(z, share), cols], s_in.at[z_me, :, cols],
                        yz_s, yz_r.at[j, 0], e_me, z * CORES + c_me,
                    )
                )
        else:
            z_send(0, s_out, s_in, share, cols, yz_s, yz_r.at[j, 0])
        s_keep[:, cols] = total

    def stage_z(j, s):
        if direct(j):
            return
        cols = chunk_cols(j)
        z_landed(zs >> s, s_in, cols.stop - cols.start, yz_r.at[j, s - 1])
        for m, owner in enumerate(z_owners(z_me, s - 1)):
            rows = z_rows(owner, share)
            total = s_keep[rows, cols] + s_in[z_slot(s - 1) + m, :, cols].astype(F32)
            s_keep[rows, cols] = total
            s_out[rows, cols] = total.astype(BF16)
        z_send(s, s_out, s_in, share, cols, yz_s, yz_r.at[j, s])

    def stage_d(j):
        cols = chunk_cols(j)
        size = cols.stop - cols.start
        total = s_keep[z_rows(z_me, share), cols]
        if direct(j):
            z_landed(zs - 1, s_in, size, yz_r.at[j, 0])
            for z in z_peers:
                total = total + s_in[z, :, cols].astype(F32)
        else:
            z_landed(1, s_in, size, yz_r.at[j, steps - 1])
            total = total + s_in[z_slot(steps - 1), :, cols].astype(F32)
        expert_out[:, cols] = total.astype(BF16)

    def mixer_final():
        z_landed(1, zin, width, mz_r.at[steps - 1])
        total = keep[z_rows(z_me, mix_share), :] + zin[z_slot(steps - 1)].astype(F32)
        mixer_out[...] = total.astype(BF16)

    lag_b, lag_c, lag_z, lag_d = LAGS
    chunks = len(CHUNKS)
    stages = [(stage_a, 0), (stage_b, lag_b), (stage_c, lag_c)]
    for s in range(1, steps):
        stages.append((functools.partial(stage_z, s=s), lag_c + s * lag_z))
    last = lag_c + (steps - 1) * lag_z + lag_d
    stages.append((stage_d, last))
    for step in range(chunks + last):
        for stage, lag in stages:
            if 0 <= step - lag < chunks:
                stage(step - lag)
        if step == 4:
            for s in range(2, steps):
                mixer_step(s)
        if step == chunks:
            mixer_final()

    everything_sent = [
        (pack.at[pl.ds(0, len(near) * half), :], near_s),
        (pack.at[pl.ds(0, len(far) * half), pl.ds(0, width // 2)], far_s),
        (pack.at[pl.ds(0, len(far) * half), pl.ds(0, width // 2)], rel_s),
        (pack.at[pl.ds(0, (ep - 1) * half), :], fwd_s),
        (wpack.at[pl.ds(0, ep - 1)], w_s),
        (pair_out, mp_s),
        (zin.at[pl.ds(0, zs - 1)], mz_s),
        (y_out, yp_s),
        (y_in.at[pl.ds(0, (ep - 1) * half), :], ye_s),
        (s_in.at[pl.ds(0, zs - 1)], yz_s),
    ]
    for ref, sem in everything_sent:
        remote(ref, ref, sem, sem, e_me, partner).wait_send()


def store(a, b, a_out, b_out, sem):
    copies = [pltpu.make_async_copy(s, d, sem.at[i]) for i, (s, d) in enumerate(((a, a_out), (b, b_out)))]
    for c in copies:
        c.start()
    for c in copies:
        c.wait()


def local(ep, tp, *args):
    (mix_tokens, mix_gain, value_w, inner_w, outer_w, taps, mix_w, moe_tokens, moe_gain,
     router_group, router_expert, routes, gate_w, up_w, down_w) = args
    rows, width = mix_tokens.shape
    count = moe_tokens.shape[0]
    channels, hidden = value_w.shape[1], gate_w.shape[2]
    experts_here = gate_w.shape[0]
    zs = tp // CORES
    side = max(s for s in range(1, ep + 1) if ep % s == 0 and s * s <= ep)
    share, mix_share = count // tp, rows // tp
    topk = routes.shape[1]
    slots = experts_here * CAP
    if experts_here % EPG == 0:
        slots = slots // topk
    slots = min(slots, share)
    half = zs * slots
    span = ep * half
    w_rows, w_cols = -(-(experts_here + 1) // 8) * 8, -(-CORES * half // 128) * 128
    chunks = len(CHUNKS)
    chunk = width // sum(CHUNKS) * max(CHUNKS)
    any_ref = pl.BlockSpec(memory_space=pl.ANY)
    vmem = pl.BlockSpec(memory_space=pltpu.VMEM)
    V, D = pltpu.VMEM, lambda *s: pltpu.SemaphoreType.DMA(s)
    one, steps = pltpu.SemaphoreType.DMA, zs.bit_length() - 1
    scratch = [
        V((1, width), F32), V(taps.shape, F32), V((1, width), F32), V(routes.T.shape, jnp.int32),
        V((rows, width), BF16), V((count, width), BF16),
        V(router_group.T.shape, BF16), V(router_expert.T.shape, BF16),
        V(value_w.shape, BF16), V(inner_w.shape, BF16), V(outer_w.shape, BF16),
        V(mix_w.shape, BF16),
        V(gate_w.shape, BF16), V(up_w.shape, BF16), V((experts_here * hidden, width), BF16),
        V((rows, width), BF16), V((count, width), BF16), V((count, 2 * span), BF16), V((2 * span, count), BF16),
        V((2 * span, width), BF16), V((2 * span, width), BF16),
        V((ep, w_rows, w_cols), F32), V((ep, w_rows, w_cols), F32), V((2 * span, w_rows), F32),
        V((rows, channels), BF16), V((16, channels), BF16), V((rows + 8, channels), F32),
        V((rows, channels), BF16), V((rows, channels), BF16),
        V((zs * mix_share, width), BF16), V((zs * mix_share, width), BF16),
        V((zs * mix_share, width), F32),
        V((zs, mix_share, width), BF16),
        V((experts_here, 2 * span, hidden), F32), V((experts_here, 2 * span, hidden), F32),
        V((2 * span, experts_here * hidden), BF16), V((2 * span, chunk), F32),
        V((span, width), BF16), V((span, width), BF16), V((span, width), F32),
        V((span, width), BF16),
        V((zs * share, width), F32), V((zs * share, width), BF16), V((zs, share, width), BF16),
        D(12), D(PARTS), one,
        one, D(PARTS), one, D(PARTS), one, D(PARTS), one, one, one, D(PARTS), one, one,
        one, one, one, D(steps), one, D(chunks), one, D(chunks), one, D(chunks, steps),
    ]
    out = [
        pltpu.VMEM((mix_share, width), BF16),
        pltpu.VMEM((share, width), BF16),
    ]
    in_specs = [any_ref] * len(args)
    results = pl.pallas_call(
        functools.partial(kernel, (ep, side, tp, zs, half, experts_here, w_rows)),
        out_shape=out,
        in_specs=in_specs,
        out_specs=[vmem, vmem],
        scratch_shapes=scratch,
        compiler_params=pltpu.CompilerParams(
            collective_id=0, has_side_effects=True, vmem_limit_bytes=65 * 1024 * 1000
        ),
        name="mixer_and_experts",
    )(
        mix_tokens, mix_gain.reshape(1, width), value_w, inner_w, outer_w, taps, mix_w,
        moe_tokens, moe_gain.reshape(1, width), router_group.T, router_expert.T, routes.T,
        gate_w, up_w, down_w,
    )
    return pl.pallas_call(
        store,
        out_shape=[jax.ShapeDtypeStruct(o.shape, BF16) for o in out],
        in_specs=[vmem, vmem],
        out_specs=[any_ref, any_ref],
        scratch_shapes=[D(2)],
        name="store",
    )(*[pltpu.with_memory_space_constraint(r, pltpu.VMEM) for r in results])


def solution(mesh):
    return jax.shard_map(
        lambda *args: tuple(local(mesh.shape["ep"], mesh.shape["tp"], *args)),
        mesh=mesh,
        in_specs=(
            P("ep", None), P(), P(None, "tp"), P(None, "tp"), P(None, "tp"), P(None, "tp"),
            P("tp", None), P("ep", None), P(), P(), P(), P("ep", None),
            P("ep", None, "tp"), P("ep", None, "tp"), P("ep", "tp", None),
        ),
        out_specs=(P(("ep", "tp"), None), P(("ep", "tp"), None)),
        check_vma=False,
    )
```

time: 50.8 us -> 47.3 us (0.931)
  Pallas kernels: 50 us -> 46.5 us
    pallas_call x2, Pallas kernels: 50 us -> 46.5 us  [the longest x1 45.8 us: local(): pl.pallas_call(functools.partial(kernel, (ep, side, tp, zs, half, experts...]
where the time goes in v1:
time: 47.3 us; the launch traced here: 47.1 us
  Pallas kernels  46.5 us (98%)
  between operations  0.64 us (1%)
    pallas_call x1, Pallas kernels, local(): pl.pallas_call(functools.partial(kernel, (ep, side, tp, zs, half, experts...  45.8 us

profile of v1, /device:TPU:0, one launch (start us, length us, event | category | flops | bytes accessed | tf_op | source)
XLA Modules:
  0.0 47.1 jit_solution(14153428029790243921)
XLA Ops:
  0.6 45.8 %mixer_and_experts.1 = (bf16[16,4096]{1,0:T(8,128)(2,1)S(1)}, bf16[16,4096]{1,0:T(8,128)(2,1)S(1)}) custom-call(bf16[128,4096]{1,0:T(8,128)(2,1)} %mix_tokens.1, f32[1,4096]{1,0:T(1,128)} %bitcast.7, bf16[4096,256]{1,0:T(8,128)(2,1)} %value_w.1, bf16[4096,256]{1,0:T(8,128)(2,1)} %inner_w.1, bf16[4096,256]{1,0:T(8,128)(2,1)} %outer_w.1, f32[3,256]{1,0:T(4,128)} %taps_in.1, ...), custom_call_target="tpu_custom_call" | custom-call | tf_op jit(solution)/shard_map/mixer_and_experts/pallas_call | solution.py:654
  46.4 0.7 %store.1 = (bf16[16,4096]{1,0:T(8,128)(2,1)}, bf16[16,4096]{1,0:T(8,128)(2,1)}) custom-call(bf16[16,4096]{1,0:T(8,128)(2,1)S(1)} %get-tuple-element.4.a, bf16[16,4096]{1,0:T(8,128)(2,1)S(1)} %get-tuple-element.5.b), custom_call_target="tpu_custom_call" | custom-call | tf_op jit(solution)/shard_map/store/pallas_call | solution.py:669

commit v2 on v1

--- a/solution.py
+++ b/solution.py
@@ -10,11 +10,12 @@
 EPG = 4
 CAP = 4
 CORES = 2
-CHUNKS = (1, 2, 2, 2, 2, 2, 2, 2, 1)
-LAGS = (2, 8, 2, 3)
-DIRECT = 2
-SPLIT = (2, 2, 3, 1)
+CHUNKS = (1, 2, 2, 2, 2, 2, 2, 1, 1, 1)
+LAGS = (1,6,2,10)
+DIRECT = 10
+SPLIT = (2, 2, 2, 2)
 PARTS = len(SPLIT)
+HOOK = 0
 MESH = pl.DeviceIdType.MESH
 F32, BF16 = jnp.float32, jnp.bfloat16
 
@@ -46,12 +47,12 @@
     return lax.rsqrt(jnp.sum(total, axis=1, keepdims=True) * (1.0 / width) + 1e-06)
 
 
-def column_tiles(width, tile, body):
+def column_tiles(first, last, tile, body):
     def step(i, carry):
         body(pl.ds(pl.multiple_of(i * tile, tile), tile))
         return carry
 
-    lax.fori_loop(0, width // tile, step, 0)
+    lax.fori_loop(first // tile, last // tile, step, 0, unroll=4)
 
 
 def kernel(
@@ -240,7 +241,10 @@
         landed(ep - 1, part_slice(q)[1], fwd_r.at[q])
 
     dispatch_far(0)
-    dispatch_near(0)
+    dispatch_far(1)
+    for q in range(2, PARTS):
+        pack_part(q)
+        dispatch_far(q)
     loads[3].wait()
     loads[10].wait()
     norm_rows(xm, mix_gain, nm)
@@ -255,14 +259,11 @@
         lax.rem(e_me + 1, ep), t_me,
     )
     halo_copy.start()
-    dispatch_far(1)
+    for q in range(PARTS - 1):
+        dispatch_near(q)
     for q in range(1, PARTS):
         for c in expert_loads(q):
             c.start()
-    for q in range(2, PARTS):
-        pack_part(q)
-        dispatch_far(q)
-        dispatch_near(q - 1)
     loads[1].wait()
     loads[2].wait()
     lanes = (((1,), (1,)), ((), ()))
@@ -384,7 +385,10 @@
             pair_out[:, cols] = both[0:mix_rows].astype(BF16)
             keep[:, cols] = both[mix_rows:]
 
-        column_tiles(width, 512, mix_tile)
+        column_tiles(0, width // 2, 512, mix_tile)
+        forward_near(0)
+        forward_far(0)
+        column_tiles(width // 2, width, 512, mix_tile)
         pair_copy.start()
 
     def mixer_sums():
@@ -395,24 +399,24 @@
             keep[:, cols] = total
             pair_in[:, cols] = total.astype(BF16)
 
-        column_tiles(width, 512, sum_tile)
-
-        z_send(0, pair_in, zin, mix_share, pl.ds(0, width), mz_s, mz_r.at[0])
-
-    def mixer_step(s):
-        z_landed(zs >> s, zin, width, mz_r.at[s - 1])
-        for m, owner in enumerate(z_owners(z_me, s - 1)):
-            rows = z_rows(owner, mix_share)
-            total = keep[rows, :] + zin[z_slot(s - 1) + m].astype(F32)
-            keep[rows, :] = total
-            pair_in[rows, :] = total.astype(BF16)
-        z_send(s, pair_in, zin, mix_share, pl.ds(0, width), mz_s, mz_r.at[s])
+        column_tiles(0, width, 512, sum_tile)
+
+        for z in z_peers:
+            start(
+                remote(
+                    pair_in.at[z_rows(z, mix_share), :], zin.at[z_me], mz_s, mz_r,
+                    e_me, z * CORES + c_me,
+                )
+            )
 
     def project(q):
         first, size = part_slice(q)
         cols = slice(first, first + size)
 
         for k in range(experts_here):
+            if k == HOOK and q + 1 < PARTS:
+                forward_near(q + 1)
+                forward_far(q + 1)
             gate = jnp.dot(got[:, cols], gw[k, cols, :], preferred_element_type=F32)
             up = jnp.dot(got[:, cols], uw[k, cols, :], preferred_element_type=F32)
             if q:
@@ -441,30 +445,18 @@
 
     for c in down_loads:
         c.start()
-    relay(0)
-    forward_near(0)
-    relay(1)
+    for q in range(PARTS):
+        relay(q)
     mixer_pair()
-    forward_far(0)
     for q in range(PARTS):
         if q == 1:
-            for later in range(2, PARTS):
-                relay(later)
             mixer_sums()
-        if q == 2:
+        if q == PARTS - 1:
             arrived_weights()
-        if q == 3:
-            mixer_step(1)
-        if 0 < q and q + 1 < PARTS:
-            forward_near(q + 1)
-            forward_far(q + 1)
         both_parts = gw.at[:, pl.ds(0, 2 * part_slice(q)[1]), :]
         pltpu.make_async_copy(both_parts, both_parts, expert_sem.at[q]).wait()
         forwarded(q)
         project(q)
-        if q == 0:
-            forward_near(1)
-            forward_far(1)
     pltpu.make_async_copy(dw, dw, down_sem).wait()
 
     chunk_unit = width // sum(CHUNKS)
@@ -553,8 +545,10 @@
         expert_out[:, cols] = total.astype(BF16)
 
     def mixer_final():
-        z_landed(1, zin, width, mz_r.at[steps - 1])
-        total = keep[z_rows(z_me, mix_share), :] + zin[z_slot(steps - 1)].astype(F32)
+        z_landed(zs - 1, zin, width, mz_r)
+        total = keep[z_rows(z_me, mix_share), :]
+        for z in z_peers:
+            total = total + zin[z].astype(F32)
         mixer_out[...] = total.astype(BF16)
 
     lag_b, lag_c, lag_z, lag_d = LAGS
@@ -568,10 +562,7 @@
         for stage, lag in stages:
             if 0 <= step - lag < chunks:
                 stage(step - lag)
-        if step == 4:
-            for s in range(2, steps):
-                mixer_step(s)
-        if step == chunks:
+        if step == chunks + lag_c - 1:
             mixer_final()
 
     everything_sent = [
@@ -644,7 +635,7 @@
         V((zs * share, width), F32), V((zs * share, width), BF16), V((zs, share, width), BF16),
         D(12), D(PARTS), one,
         one, D(PARTS), one, D(PARTS), one, D(PARTS), one, one, one, D(PARTS), one, one,
-        one, one, one, D(steps), one, D(chunks), one, D(chunks), one, D(chunks, steps),
+        one, one, one, one, one, D(chunks), one, D(chunks), one, D(chunks, steps),
     ]
     out = [
         pltpu.VMEM((mix_share, width), BF16),

time: 47.3 us -> 42.5 us (0.90)
  Pallas kernels: 46.5 us -> 41.7 us
    pallas_call x1, Pallas kernels: 45.8 us -> 41 us  [local(): pl.pallas_call(functools.partial(kernel, (ep, side, tp, zs, half, experts...]
where the time goes in v2:
time: 42.5 us; the launch traced here: 42.3 us
  Pallas kernels  41.7 us (98%)
  between operations  0.64 us (2%)
    pallas_call x1, Pallas kernels, local(): pl.pallas_call(functools.partial(kernel, (ep, side, tp, zs, half, experts...  41 us

profile of v2, /device:TPU:0, one launch (start us, length us, event | category | flops | bytes accessed | tf_op | source)
XLA Modules:
  0.0 42.3 jit_solution(11634098709726191701)
XLA Ops:
  0.6 41.0 %mixer_and_experts.1 = (bf16[16,4096]{1,0:T(8,128)(2,1)S(1)}, bf16[16,4096]{1,0:T(8,128)(2,1)S(1)}) custom-call(bf16[128,4096]{1,0:T(8,128)(2,1)} %mix_tokens.1, f32[1,4096]{1,0:T(1,128)} %bitcast.7, bf16[4096,256]{1,0:T(8,128)(2,1)} %value_w.1, bf16[4096,256]{1,0:T(8,128)(2,1)} %inner_w.1, bf16[4096,256]{1,0:T(8,128)(2,1)} %outer_w.1, f32[3,256]{1,0:T(4,128)} %taps_in.1, ...), custom_call_target="tpu_custom_call" | custom-call | tf_op jit(solution)/shard_map/mixer_and_experts/pallas_call | solution.py:645
  41.6 0.7 %store.1 = (bf16[16,4096]{1,0:T(8,128)(2,1)}, bf16[16,4096]{1,0:T(8,128)(2,1)}) custom-call(bf16[16,4096]{1,0:T(8,128)(2,1)S(1)} %get-tuple-element.4.a, bf16[16,4096]{1,0:T(8,128)(2,1)S(1)} %get-tuple-element.5.b), custom_call_target="tpu_custom_call" | custom-call | tf_op jit(solution)/shard_map/store/pallas_call | solution.py:660

commit v3 on v2

--- a/solution.py
+++ b/solution.py
@@ -10,9 +10,8 @@
 EPG = 4
 CAP = 4
 CORES = 2
-CHUNKS = (1, 2, 2, 2, 2, 2, 2, 1, 1, 1)
-LAGS = (1,6,2,10)
-DIRECT = 10
+CHUNKS = (1, 3, 4, 4, 4, 4, 4, 4, 2, 2)
+LAGS = (1, 6)
 SPLIT = (2, 2, 2, 2)
 PARTS = len(SPLIT)
 HOOK = 0
@@ -85,7 +84,15 @@
     ep_peers = near + far
     z_odd = lax.rem(z_me, 2)
     z_pair = z_me + 1 - 2 * z_odd
-    z_peers = [lax.rem(z_me + d, zs) for d in range(1, zs)]
+
+    def z_flipped(bits):
+        z = z_me
+        for b in range(zs.bit_length() - 1):
+            if bits >> b & 1:
+                z = z + (1 - 2 * lax.rem(z_me // 2**b, 2)) * 2**b
+        return z
+
+    z_peers = [z_flipped(bits) for bits in range(zs - 1, 0, -1)]
 
     def start(copy):
         copy.start()
@@ -259,8 +266,7 @@
         lax.rem(e_me + 1, ep), t_me,
     )
     halo_copy.start()
-    for q in range(PARTS - 1):
-        dispatch_near(q)
+    dispatch_near(0)
     for q in range(1, PARTS):
         for c in expert_loads(q):
             c.start()
@@ -317,7 +323,8 @@
 
     for e in ep_peers:
         start(remote(wpack.at[e], wgot.at[e_me], w_s, w_r, e, t_me))
-    dispatch_near(PARTS - 1)
+    for q in range(1, PARTS):
+        dispatch_near(q)
     padded[8:, :] = gated[...].astype(F32)
     loads[6].wait()
     outer_proj = jnp.dot(nm[...], ow[...], preferred_element_type=F32)
@@ -337,28 +344,6 @@
 
     def z_rows(z, step):
         return pl.ds(pl.multiple_of(z * step, step), step)
-
-    steps = zs.bit_length() - 1
-
-    def z_partner(s):
-        return z_me + (1 - 2 * lax.rem(z_me // 2**s, 2)) * 2**s
-
-    def z_owners(z, s):
-        low = lax.rem(z, 2 ** (s + 1))
-        return [low + m * 2 ** (s + 1) for m in range(zs >> (s + 1))]
-
-    def z_slot(s):
-        return sum(zs >> (t + 1) for t in range(s))
-
-    def z_send(s, src, dst, step, cols, s_sem, r_sem):
-        to = z_partner(s)
-        for m, owner in enumerate(z_owners(to, s)):
-            start(
-                remote(
-                    src.at[z_rows(owner, step), cols], dst.at[z_slot(s) + m, :, cols],
-                    s_sem, r_sem, e_me, to * CORES + c_me,
-                )
-            )
 
     def z_landed(blocks, ref, size, sem):
         here = ref.at[pl.ds(0, blocks), :, pl.ds(0, size)]
@@ -449,13 +434,13 @@
         relay(q)
     mixer_pair()
     for q in range(PARTS):
-        if q == 1:
-            mixer_sums()
-        if q == PARTS - 1:
+        if q == 0:
             arrived_weights()
         both_parts = gw.at[:, pl.ds(0, 2 * part_slice(q)[1]), :]
         pltpu.make_async_copy(both_parts, both_parts, expert_sem.at[q]).wait()
         forwarded(q)
+        if q == 0:
+            mixer_sums()
         project(q)
     pltpu.make_async_copy(dw, dw, down_sem).wait()
 
@@ -472,6 +457,16 @@
     def stage_a(j):
         cols = chunk_cols(j)
         size = cols.stop - cols.start
+        if j == 0:
+            for c, dst in ((c_no, y_out), (c_me, y_keep)):
+                part = jnp.dot(hid[core_rows(c), :], dw[:, cols], preferred_element_type=F32)
+                dst[:, cols] = part.astype(dst.dtype)
+                if dst is y_out:
+                    y_copies[j] = remote(
+                        y_out.at[:, cols], y_in.at[:, cols], yp_s, yp_r.at[j], e_me, partner
+                    )
+                    y_copies[j].start()
+            return
         both_y[:, 0:size] = jnp.dot(hid[...], dw[:, cols], preferred_element_type=F32)
         y_out[:, cols] = both_y[core_rows(c_no), 0:size].astype(BF16)
         y_keep[:, cols] = both_y[core_rows(c_me), 0:size]
@@ -487,7 +482,7 @@
         cols = chunk_cols(j)
         y_copies[j].wait_recv()
         y_in[:, cols] = (y_keep[:, cols] + y_in[:, cols].astype(F32)).astype(BF16)
-        for e in ep_peers:
+        for e in far + near:
             start(
                 remote(
                     y_in.at[e_rows(e), cols], e_in.at[e_rows(e_me), cols],
@@ -495,9 +490,6 @@
                 )
             )
         e_in[e_rows(e_me), cols] = y_in[e_rows(e_me), cols]
-
-    def direct(j):
-        return j >= len(CHUNKS) - DIRECT
 
     def stage_c(j):
         cols = chunk_cols(j)
@@ -507,41 +499,21 @@
         own = parity_rows(spread, c_me, share, core_rows(c_me))
         total = jnp.dot(own, e_in[:, cols], preferred_element_type=F32)
         s_out[:, cols] = total.astype(BF16)
-        if direct(j):
-            for z in z_peers:
-                start(
-                    remote(
-                        s_out.at[z_rows(z, share), cols], s_in.at[z_me, :, cols],
-                        yz_s, yz_r.at[j, 0], e_me, z * CORES + c_me,
-                    )
+        for z in z_peers:
+            start(
+                remote(
+                    s_out.at[z_rows(z, share), cols], s_in.at[z_me, :, cols],
+                    yz_s, yz_r.at[j], e_me, z * CORES + c_me,
                 )
-        else:
-            z_send(0, s_out, s_in, share, cols, yz_s, yz_r.at[j, 0])
+            )
         s_keep[:, cols] = total
-
-    def stage_z(j, s):
-        if direct(j):
-            return
-        cols = chunk_cols(j)
-        z_landed(zs >> s, s_in, cols.stop - cols.start, yz_r.at[j, s - 1])
-        for m, owner in enumerate(z_owners(z_me, s - 1)):
-            rows = z_rows(owner, share)
-            total = s_keep[rows, cols] + s_in[z_slot(s - 1) + m, :, cols].astype(F32)
-            s_keep[rows, cols] = total
-            s_out[rows, cols] = total.astype(BF16)
-        z_send(s, s_out, s_in, share, cols, yz_s, yz_r.at[j, s])
 
     def stage_d(j):
         cols = chunk_cols(j)
-        size = cols.stop - cols.start
+        z_landed(zs - 1, s_in, cols.stop - cols.start, yz_r.at[j])
         total = s_keep[z_rows(z_me, share), cols]
-        if direct(j):
-            z_landed(zs - 1, s_in, size, yz_r.at[j, 0])
-            for z in z_peers:
-                total = total + s_in[z, :, cols].astype(F32)
-        else:
-            z_landed(1, s_in, size, yz_r.at[j, steps - 1])
-            total = total + s_in[z_slot(steps - 1), :, cols].astype(F32)
+        for z in z_peers:
+            total = total + s_in[z, :, cols].astype(F32)
         expert_out[:, cols] = total.astype(BF16)
 
     def mixer_final():
@@ -551,14 +523,10 @@
             total = total + zin[z].astype(F32)
         mixer_out[...] = total.astype(BF16)
 
-    lag_b, lag_c, lag_z, lag_d = LAGS
+    lag_b, lag_c = LAGS
     chunks = len(CHUNKS)
-    stages = [(stage_a, 0), (stage_b, lag_b), (stage_c, lag_c)]
-    for s in range(1, steps):
-        stages.append((functools.partial(stage_z, s=s), lag_c + s * lag_z))
-    last = lag_c + (steps - 1) * lag_z + lag_d
-    stages.append((stage_d, last))
-    for step in range(chunks + last):
+    stages = [(stage_a, 0), (stage_b, lag_b), (stage_c, lag_c), (stage_d, lag_c + chunks)]
+    for step in range(2 * chunks + lag_c):
         for stage, lag in stages:
             if 0 <= step - lag < chunks:
                 stage(step - lag)
@@ -612,7 +580,7 @@
     any_ref = pl.BlockSpec(memory_space=pl.ANY)
     vmem = pl.BlockSpec(memory_space=pltpu.VMEM)
     V, D = pltpu.VMEM, lambda *s: pltpu.SemaphoreType.DMA(s)
-    one, steps = pltpu.SemaphoreType.DMA, zs.bit_length() - 1
+    one = pltpu.SemaphoreType.DMA
     scratch = [
         V((1, width), F32), V(taps.shape, F32), V((1, width), F32), V(routes.T.shape, jnp.int32),
         V((rows, width), BF16), V((count, width), BF16),
@@ -635,7 +603,7 @@
         V((zs * share, width), F32), V((zs * share, width), BF16), V((zs, share, width), BF16),
         D(12), D(PARTS), one,
         one, D(PARTS), one, D(PARTS), one, D(PARTS), one, one, one, D(PARTS), one, one,
-        one, one, one, one, one, D(chunks), one, D(chunks), one, D(chunks, steps),
+        one, one, one, one, one, D(chunks), one, D(chunks), one, D(chunks),
     ]
     out = [
         pltpu.VMEM((mix_share, width), BF16),

time: 42.5 us -> 42 us (0.988)
  Pallas kernels: 41.7 us -> 41.2 us
    pallas_call x1, Pallas kernels: 41 us -> 40.4 us  [local(): pl.pallas_call(functools.partial(kernel, (ep, side, tp, zs, half, experts...]
where the time goes in v3:
time: 42 us; the launch traced here: 41.8 us
  Pallas kernels  41.2 us (98%)
  between operations  0.64 us (2%)
    pallas_call x1, Pallas kernels, local(): pl.pallas_call(functools.partial(kernel, (ep, side, tp, zs, half, experts...  40.4 us

profile of v3, /device:TPU:0, one launch (start us, length us, event | category | flops | bytes accessed | tf_op | source)
XLA Modules:
  0.0 41.8 jit_solution(2812410097520668546)
XLA Ops:
  0.6 40.4 %mixer_and_experts.1 = (bf16[16,4096]{1,0:T(8,128)(2,1)S(1)}, bf16[16,4096]{1,0:T(8,128)(2,1)S(1)}) custom-call(bf16[128,4096]{1,0:T(8,128)(2,1)} %mix_tokens.1, f32[1,4096]{1,0:T(1,128)} %bitcast.7, bf16[4096,256]{1,0:T(8,128)(2,1)} %value_w.1, bf16[4096,256]{1,0:T(8,128)(2,1)} %inner_w.1, bf16[4096,256]{1,0:T(8,128)(2,1)} %outer_w.1, f32[3,256]{1,0:T(4,128)} %taps_in.1, ...), custom_call_target="tpu_custom_call" | custom-call | tf_op jit(solution)/shard_map/mixer_and_experts/pallas_call | solution.py:613
  41.1 0.7 %store.1 = (bf16[16,4096]{1,0:T(8,128)(2,1)}, bf16[16,4096]{1,0:T(8,128)(2,1)}) custom-call(bf16[16,4096]{1,0:T(8,128)(2,1)S(1)} %get-tuple-element.4.a, bf16[16,4096]{1,0:T(8,128)(2,1)S(1)} %get-tuple-element.5.b), custom_call_target="tpu_custom_call" | custom-call | tf_op jit(solution)/shard_map/store/pallas_call | solution.py:628

commit v4 on v3

--- a/solution.py
+++ b/solution.py
@@ -14,7 +14,7 @@
 LAGS = (1, 6)
 SPLIT = (2, 2, 2, 2)
 PARTS = len(SPLIT)
-HOOK = 0
+HOOK = 1
 MESH = pl.DeviceIdType.MESH
 F32, BF16 = jnp.float32, jnp.bfloat16
 

time: 42 us -> 42.8 us (1.019)
  Pallas kernels: 41.2 us -> 41.9 us
    pallas_call x1, Pallas kernels: 40.4 us -> 41.2 us  [local(): pl.pallas_call(functools.partial(kernel, (ep, side, tp, zs, half, experts...]
where the time goes in v4:
time: 42.8 us; the launch traced here: 42.6 us
  Pallas kernels  41.9 us (98%)
  between operations  0.64 us (1%)
    pallas_call x1, Pallas kernels, local(): pl.pallas_call(functools.partial(kernel, (ep, side, tp, zs, half, experts...  41.2 us

profile of v4, /device:TPU:0, one launch (start us, length us, event | category | flops | bytes accessed | tf_op | source)
XLA Modules:
  0.0 42.6 jit_solution(14984795549654084010)
XLA Ops:
  0.6 41.2 %mixer_and_experts.1 = (bf16[16,4096]{1,0:T(8,128)(2,1)S(1)}, bf16[16,4096]{1,0:T(8,128)(2,1)S(1)}) custom-call(bf16[128,4096]{1,0:T(8,128)(2,1)} %mix_tokens.1, f32[1,4096]{1,0:T(1,128)} %bitcast.7, bf16[4096,256]{1,0:T(8,128)(2,1)} %value_w.1, bf16[4096,256]{1,0:T(8,128)(2,1)} %inner_w.1, bf16[4096,256]{1,0:T(8,128)(2,1)} %outer_w.1, f32[3,256]{1,0:T(4,128)} %taps_in.1, ...), custom_call_target="tpu_custom_call" | custom-call | tf_op jit(solution)/shard_map/mixer_and_experts/pallas_call | solution.py:613
  41.9 0.7 %store.1 = (bf16[16,4096]{1,0:T(8,128)(2,1)}, bf16[16,4096]{1,0:T(8,128)(2,1)}) custom-call(bf16[16,4096]{1,0:T(8,128)(2,1)S(1)} %get-tuple-element.4.a, bf16[16,4096]{1,0:T(8,128)(2,1)S(1)} %get-tuple-element.5.b), custom_call_target="tpu_custom_call" | custom-call | tf_op jit(solution)/shard_map/store/pallas_call | solution.py:628
